TPU v7x, 32 devices: a whole 2x2x4 slice. The times are simulated.
32 devices in a mesh: sp: 8 (over z, x), tp: 4 (over y, core).
Axes of the slice: x: 2, y: 2, z: 4, core: 2. Of those that a mesh axis runs over, the one named last changes fastest.
Arguments:
- hidden_states: bfloat16 [6144, 4096], P('sp'), may hold values from -60 to 60
- w_conv_b: bfloat16 [4096, 2048], P(None, 'tp'), may hold values from -0.09375 to 0.09375
- w_conv_c: bfloat16 [4096, 2048], P(None, 'tp'), may hold values from -0.09375 to 0.09375
- w_conv_h: bfloat16 [4096, 2048], P(None, 'tp'), may hold values from -0.09375 to 0.09375
- conv_taps: bfloat16 [3, 2048], P(None, 'tp'), may hold values from -3.5 to 3.5
- w_query: bfloat16 [4096, 2048], P(None, 'tp'), may hold values from -0.15625 to 0.15625
- w_key: bfloat16 [4096, 2048], P(None, 'tp'), may hold values from -0.09375 to 0.09375
- w_value: bfloat16 [4096, 2048], P(None, 'tp'), may hold values from -0.09375 to 0.09375
- lambdas: float32 [16], P('tp'), may hold values from 0.3 to 0.8
- head_gain: bfloat16 [128], replicated, may hold values from 0.099609375 to 1.8984375
- w_out_conv: bfloat16 [2048, 4096], P('tp'), may hold values from -1 to 1
- w_out_attn: bfloat16 [2048, 4096], P('tp'), may hold values from -1 to 1
- out_gain: bfloat16 [4096], replicated, may hold values from 0.099609375 to 1.8984375
Outputs:
- mixed: bfloat16 [6144, 4096], P('sp', 'tp')
All inputs are finite; a program needn't handle non-finite values.
Results may differ from a plain program's by a relative error of at most 0.023.
Values may be sent and summed in bfloat16 or wider, within the bound.
A program may use at most 192 MiB of HBM per device.

v0:
```python
import jax
import jax.numpy as jnp
from jax import lax
from jax.sharding import PartitionSpec as P

D = 4096
QK = 64
TAPS = 3
VD = 128
NEG_LARGE = -1e30


def passed_along(block, axis, distance):
    devices = range(lax.axis_size(axis))
    route = [(i - distance, i) for i in devices if i - distance in devices]
    return lax.ppermute(block, axis, route)


def rotate(values, positions):
    inverse = 1.0 / 10000.0 ** (jnp.arange(0, QK, 2, dtype=jnp.float32) / QK)
    angles = positions[:, None] * inverse[None, :]
    angles = jnp.concatenate([angles, angles], axis=-1)
    cosine = jnp.cos(angles)[:, None, None, :]
    sine = jnp.sin(angles)[:, None, None, :]
    first_half, second_half = jnp.split(values, 2, axis=-1)
    return values * cosine + jnp.concatenate([-second_half, first_half], axis=-1) * sine


def per_device(
    hidden_states,
    w_conv_b,
    w_conv_c,
    w_conv_h,
    conv_taps,
    w_query,
    w_key,
    w_value,
    lambdas,
    head_gain,
    w_out_conv,
    w_out_attn,
    out_gain,
):
    tok_rows = hidden_states.shape[0]
    head_count = w_value.shape[1] // VD
    channels = w_conv_b.shape[1]
    offset = lax.axis_index("sp") * tok_rows
    query_pos = offset + jnp.arange(tok_rows, dtype=jnp.int32)
    positions = query_pos.astype(jnp.float32)

    def project(weight):
        return jnp.dot(hidden_states, weight, preferred_element_type=jnp.float32).astype(
            jnp.bfloat16
        )

    key_rot = rotate(
        project(w_key).reshape(tok_rows, head_count, 2, QK).astype(jnp.float32), positions
    ).astype(jnp.bfloat16)
    values = project(w_value)
    query_rot = rotate(
        project(w_query).reshape(tok_rows, head_count, 2, QK).astype(jnp.float32), positions
    ).astype(jnp.bfloat16)
    scale = QK ** (-0.5)

    def attend(state, keys_blk, vals_blk, first_pos):
        running_max, running_sum, numer = state
        scores = (
            jnp.einsum("qhcd,khcd->hcqk", query_rot, keys_blk, preferred_element_type=jnp.float32)
            * scale
        )
        key_pos = first_pos + jnp.arange(keys_blk.shape[0], dtype=jnp.int32)
        visible = (key_pos[None, :] <= query_pos[:, None])[None, None]
        scores = jnp.where(visible, scores, NEG_LARGE)
        new_max = jnp.maximum(running_max, jnp.max(scores, axis=-1))
        weights = jnp.where(visible, jnp.exp(scores - new_max[..., None]), 0.0)
        factor = jnp.exp(running_max - new_max)
        running_sum = running_sum * factor + jnp.sum(weights, axis=-1)
        numer = numer * factor[..., None] + jnp.einsum(
            "hcqk,khe->hcqe",
            weights.astype(jnp.bfloat16),
            vals_blk,
            preferred_element_type=jnp.float32,
        )
        return (new_max, running_sum, numer)

    initial = (
        jnp.full((head_count, 2, tok_rows), NEG_LARGE, jnp.float32),
        jnp.zeros((head_count, 2, tok_rows), jnp.float32),
        jnp.zeros((head_count, 2, tok_rows, VD), jnp.float32),
    )
    packed_keys = key_rot.reshape(tok_rows, head_count * 2 * QK)
    key_piece = lax.all_gather(packed_keys, "sp", axis=0, tiled=True)
    value_piece = lax.all_gather(values, "sp", axis=0, tiled=True)
    count = key_piece.shape[0]
    block = 512

    def one_block(index, state):
        first = index * block
        keys_blk = lax.dynamic_slice_in_dim(key_piece, first, block, 0).reshape(
            block, head_count, 2, QK
        )
        vals_blk = lax.dynamic_slice_in_dim(value_piece, first, block, 0).reshape(
            block, head_count, VD
        )
        return attend(state, keys_blk, vals_blk, first)

    def work(state):
        return lax.fori_loop(0, count // block, one_block, state)

    running_max, running_sum, numer = lax.cond(
        jnp.int32(0) <= offset + tok_rows - 1, work, lambda state: state, initial
    )
    u_b = project(w_conv_b)
    u_c = project(w_conv_c)
    u_h = project(w_conv_h)
    gated = u_c.astype(jnp.float32) * u_h.astype(jnp.float32)
    rim_rows = passed_along(gated[tok_rows - (TAPS - 1) :], "sp", 1)
    padded = jnp.concatenate([rim_rows, gated], axis=0)
    taps_f = conv_taps.astype(jnp.float32)
    convolved = jnp.zeros((tok_rows, channels), jnp.float32)
    for tap in range(TAPS):
        convolved = convolved + taps_f[tap][None, :] * padded[tap : tap + tok_rows]
    conv_out = (u_b.astype(jnp.float32) * convolved).astype(jnp.bfloat16)
    diff = (
        numer[:, 0] / running_sum[:, 0, :, None]
        - lambdas[:, None, None] * numer[:, 1] / running_sum[:, 1, :, None]
    )
    normed = (
        diff
        * lax.rsqrt(jnp.mean(diff * diff, axis=-1, keepdims=True) + 1e-05)
        * head_gain.astype(jnp.float32)[None, None, :]
    )
    attn_out = normed.astype(jnp.bfloat16).transpose(1, 0, 2).reshape(tok_rows, head_count * VD)
    gain_f = out_gain.astype(jnp.float32)
    partial_value = jnp.dot(conv_out, w_out_conv, preferred_element_type=jnp.float32) + jnp.dot(
        attn_out, w_out_attn, preferred_element_type=jnp.float32
    )
    summed = lax.psum_scatter(
        partial_value.astype(jnp.bfloat16), "tp", scatter_dimension=1, tiled=True
    )
    mix_f = summed.astype(jnp.float32)
    width = mix_f.shape[1]
    total_sum, total_squares = lax.psum(
        (jnp.sum(mix_f, axis=-1), jnp.sum(mix_f * mix_f, axis=-1)), "tp"
    )
    mean_value = (total_sum / D)[:, None]
    variance = (total_squares / D)[:, None] - mean_value * mean_value
    own_gain = lax.dynamic_slice_in_dim(gain_f, lax.axis_index("tp") * width, width, 0)
    return ((mix_f - mean_value) * lax.rsqrt(variance + 1e-05) * own_gain[None, :]).astype(
        jnp.bfloat16
    )


def solution(mesh):
    return jax.shard_map(
        per_device,
        mesh=mesh,
        in_specs=(
            P("sp", None),
            P(None, "tp"),
            P(None, "tp"),
            P(None, "tp"),
            P(None, "tp"),
            P(None, "tp"),
            P(None, "tp"),
            P(None, "tp"),
            P("tp"),
            P(),
            P("tp", None),
            P("tp", None),
            P(),
        ),
        out_specs=P("sp", "tp"),
        check_vma=False,
    )
```

profile of v0, /device:TPU:0, one launch (start us, length us, event | category | flops | bytes accessed | tf_op | source)
XLA Modules:
  0.0 625.5 jit_solution(7716799668903363379)
XLA Ops:
  6.6 7.6 %convolution_convert_fusion.1 = bf16[768,512]{0,1:T(8,128)(2,1)S(1)} fusion(bf16[768,4096]{1,0:T(8,128)(2,1)} %param.17, bf16[4096,512]{1,0:T(8,128)(2,1)} %param.22), kind=kOutput, calls=%fused_computation.57 | convolution fusion | flops 3221618688 | bytes 11272192 | tf_op jit(solution)/shard_map/dot_general | solution.py:52
  24.7 8.3 %convolution_convert_fusion = bf16[768,512]{1,0:T(8,128)(2,1)} fusion(bf16[768,4096]{1,0:T(8,128)(2,1)} %param.17, bf16[4096,512]{1,0:T(8,128)(2,1)} %param.24), kind=kOutput, calls=%fused_computation.56 | convolution fusion | flops 3221618688 | bytes 11272192 | tf_op jit(solution)/shard_map/dot_general | solution.py:52
  33.3 8.4 %convolution_convert_fusion.3 = bf16[768,512]{1,0:T(8,128)(2,1)S(1)} fusion(bf16[768,4096]{1,0:T(8,128)(2,1)} %param.17, bf16[4096,512]{1,0:T(8,128)(2,1)} %param.20), kind=kOutput, calls=%fused_computation.60 | convolution fusion | flops 3221618688 | bytes 11272192 | tf_op jit(solution)/shard_map/dot_general | solution.py:52
  41.7 5.5 convert_multiply_fusion.1
  53.2 15.1 %fusion.33 = f32[768,4096]{1,0:T(8,128)} fusion(bf16[512,4096]{1,0:T(8,128)(2,1)} %param.27, f32[2,512]{1,0:T(2,128)S(1)} %collective-permute-done, f32[768,512]{1,0:T(8,128)} %copy-done.2, bf16[768,4096]{1,0:T(8,128)(2,1)} %param.17, bf16[4096,512]{1,0:T(8,128)(2,1)} %param.18, f32[512]{0:T(512)S(1)} %bitcast.103, f32[512]{0:T(512)S(1)} %bitcast.102, ...), kind=kOutput, calls=%fused_computation.65 | convolution fusion | flops 6446776320 | bytes 28846080 | tf_op jit(solution)/shard_map/dot_general | solution.py:135
  68.3 57.8 %all-gather.3.cloned.1.call-done = bf16[6144,512]{0,1:T(8,128)(2,1)} async-done(((bf16[768,512]{0,1:T(8,128)(2,1)}), bf16[6144,512]{0,1:T(8,128)(2,1)}) %all-gather.3.cloned.1.call-update) | async-done | bytes 6291472 | tf_op jit(solution)/shard_map/all_gather | solution.py:92
  126.0 99.4 %all-gather.5.cloned.1.call-done = bf16[6144,512]{1,0:T(8,128)(2,1)} async-done(((bf16[768,512]{1,0:T(8,128)(2,1)}), bf16[6144,512]{1,0:T(8,128)(2,1)}) %all-gather.5.cloned.1.call-update) | async-done | bytes 6291472 | tf_op jit(solution)/shard_map/all_gather | solution.py:93
  225.5 312.6 %conditional.1 = (f32[4,2,768]{2,1,0:T(2,128)}, f32[4,2,768,128]{3,2,1,0:T(8,128)}) conditional(s32[]{:T(128)} %convert_element_type.98, () %tuple.27, (s32[]{:T(128)}, s32[768]{0:T(1024)S(1)}, bf16[6144,512]{0,1:T(8,128)(2,1)}, bf16[768,4,2,64]{0,3,2,1:T(8,128)(2,1)S(1)}, bf16[6144,512]{1,0:T(8,128)(2,1)}) %tuple.28), branch_computations={%region_0.0_spmd, %region_1.6_spmd} | conditional | flops 1251638528 | bytes 51000628 | solution.py:110
  225.5 312.6 %while.17 = (s32[]{:T(128)}, f32[4,2,768]{2,1,0:T(2,128)S(1)}, f32[4,2,768]{2,1,0:T(2,128)}, f32[4,2,768,128]{3,2,1,0:T(8,128)}, s32[768]{0:T(1024)S(1)}, /*inde...) while((s32[]{:T(128)}, f32[4,2,768]{2,1,0:T(2,128)S(1)}, ...), condition=%wide.region_5.5_spmd.clone, body=%wide.region_2.4_spmd.clone.sunk | while | flops 1251637760 | bytes 50994360 | solution.py:108
  226.9 6.6 %fusion.71 = (f32[4,2,768]{2,1,0:T(2,128)S(1)}, f32[4,2,512,768]{3,2,1,0:T(8,128)}) fusion(pred[768,512]{0,1:T(8,128)(4,1)S(1)} %broadcast_compare_fusion.2, bf16[512,4,2,64]{0,3,2,1:T(8,128)(2,1)S(1)} %bitcast.92, bf16[768,4,2,64]{0,3,2,1:T(8,128)(2,1)S(1)} %get-tuple-element.325), kind=kOutput, calls=%fused_computation.2.clone.1 | convolution fusion | flops 412084224 | bytes 14311424 | tf_op jit(solution)/shard_map/cond/branch_1_fun/while/body/eval_jaxpr/qhcd,khcd->hcqk/dot_general | solution.py:68
  233.5 6.5 %fusion.73 = f32[4,2,768]{2,1,0:T(2,128)S(1)} fusion(f32[4,2,512,768]{3,2,1,0:T(8,128)} %get-tuple-element.292, f32[4,2,768]{2,1,0:T(2,128)S(1)} %fusion.72, pred[768,512]{0,1:T(8,128)(4,1)S(1)} %broadcast_compare_fusion.2), kind=kLoop, calls=%fused_computation.4.clone.1 | loop fusion | flops 15722496 | bytes 13025280 | tf_op jit(solution)/shard_map/cond/branch_1_fun/while/body/eval_jaxpr/reduce_sum | solution.py:77
  241.9 8.5 %fusion.75 = f32[4,2,768,128]{3,2,1,0:T(8,128)} fusion(f32[4,2,768,128]{3,2,1,0:T(8,128)} %get-tuple-element.310, bf16[512,4,128,1]{0,2,3,1:T(8,128)(2,1)S(1)} %bitcast.93, f32[4,2,512,768]{3,2,1,0:T(8,128)} %get-tuple-element.292, f32[4,2,768]{2,1,0:T(2,128)S(1)} %fusion.72, pred[768,512]{0,1:T(8,128)(4,1)S(1)} %broadcast_compare_fusion.2, ...), kind=kOutput, calls=%fused_computation.8.clone.1 | convolution fusion | flops 823394304 | bytes 19841024 | tf_op jit(solution)/shard_map/cond/branch_1_fun/while/body/eval_jaxpr/hcqk,khe->hcqe/dot_general | solution.py:78
  251.8 6.6 %fusion.71 = (f32[4,2,768]{2,1,0:T(2,128)S(1)}, f32[4,2,512,768]{3,2,1,0:T(8,128)}) fusion(pred[768,512]{0,1:T(8,128)(4,1)S(1)} %broadcast_compare_fusion.2, bf16[512,4,2,64]{0,3,2,1:T(8,128)(2,1)S(1)} %bitcast.92, bf16[768,4,2,64]{0,3,2,1:T(8,128)(2,1)S(1)} %get-tuple-element.325), kind=kOutput, calls=%fused_computation.2.clone.1 | convolution fusion | flops 412084224 | bytes 14311424 | tf_op jit(solution)/shard_map/cond/branch_1_fun/while/body/eval_jaxpr/qhcd,khcd->hcqk/dot_general | solution.py:68
  258.4 6.5 %fusion.73 = f32[4,2,768]{2,1,0:T(2,128)S(1)} fusion(f32[4,2,512,768]{3,2,1,0:T(8,128)} %get-tuple-element.292, f32[4,2,768]{2,1,0:T(2,128)S(1)} %fusion.72, pred[768,512]{0,1:T(8,128)(4,1)S(1)} %broadcast_compare_fusion.2), kind=kLoop, calls=%fused_computation.4.clone.1 | loop fusion | flops 15722496 | bytes 13025280 | tf_op jit(solution)/shard_map/cond/branch_1_fun/while/body/eval_jaxpr/reduce_sum | solution.py:77
  267.6 9.0 %fusion.75 = f32[4,2,768,128]{3,2,1,0:T(8,128)} fusion(f32[4,2,768,128]{3,2,1,0:T(8,128)} %get-tuple-element.310, bf16[512,4,128,1]{0,2,3,1:T(8,128)(2,1)S(1)} %bitcast.93, f32[4,2,512,768]{3,2,1,0:T(8,128)} %get-tuple-element.292, f32[4,2,768]{2,1,0:T(2,128)S(1)} %fusion.72, pred[768,512]{0,1:T(8,128)(4,1)S(1)} %broadcast_compare_fusion.2, ...), kind=kOutput, calls=%fused_computation.8.clone.1 | convolution fusion | flops 823394304 | bytes 19841024 | tf_op jit(solution)/shard_map/cond/branch_1_fun/while/body/eval_jaxpr/hcqk,khe->hcqe/dot_general | solution.py:78
  278.0 6.6 %fusion.71 = (f32[4,2,768]{2,1,0:T(2,128)S(1)}, f32[4,2,512,768]{3,2,1,0:T(8,128)}) fusion(pred[768,512]{0,1:T(8,128)(4,1)S(1)} %broadcast_compare_fusion.2, bf16[512,4,2,64]{0,3,2,1:T(8,128)(2,1)S(1)} %bitcast.92, bf16[768,4,2,64]{0,3,2,1:T(8,128)(2,1)S(1)} %get-tuple-element.325), kind=kOutput, calls=%fused_computation.2.clone.1 | convolution fusion | flops 412084224 | bytes 14311424 | tf_op jit(solution)/shard_map/cond/branch_1_fun/while/body/eval_jaxpr/qhcd,khcd->hcqk/dot_general | solution.py:68
  284.6 6.5 %fusion.73 = f32[4,2,768]{2,1,0:T(2,128)S(1)} fusion(f32[4,2,512,768]{3,2,1,0:T(8,128)} %get-tuple-element.292, f32[4,2,768]{2,1,0:T(2,128)S(1)} %fusion.72, pred[768,512]{0,1:T(8,128)(4,1)S(1)} %broadcast_compare_fusion.2), kind=kLoop, calls=%fused_computation.4.clone.1 | loop fusion | flops 15722496 | bytes 13025280 | tf_op jit(solution)/shard_map/cond/branch_1_fun/while/body/eval_jaxpr/reduce_sum | solution.py:77
  293.8 9.0 %fusion.75 = f32[4,2,768,128]{3,2,1,0:T(8,128)} fusion(f32[4,2,768,128]{3,2,1,0:T(8,128)} %get-tuple-element.310, bf16[512,4,128,1]{0,2,3,1:T(8,128)(2,1)S(1)} %bitcast.93, f32[4,2,512,768]{3,2,1,0:T(8,128)} %get-tuple-element.292, f32[4,2,768]{2,1,0:T(2,128)S(1)} %fusion.72, pred[768,512]{0,1:T(8,128)(4,1)S(1)} %broadcast_compare_fusion.2, ...), kind=kOutput, calls=%fused_computation.8.clone.1 | convolution fusion | flops 823394304 | bytes 19841024 | tf_op jit(solution)/shard_map/cond/branch_1_fun/while/body/eval_jaxpr/hcqk,khe->hcqe/dot_general | solution.py:78
  304.1 6.6 %fusion.71 = (f32[4,2,768]{2,1,0:T(2,128)S(1)}, f32[4,2,512,768]{3,2,1,0:T(8,128)}) fusion(pred[768,512]{0,1:T(8,128)(4,1)S(1)} %broadcast_compare_fusion.2, bf16[512,4,2,64]{0,3,2,1:T(8,128)(2,1)S(1)} %bitcast.92, bf16[768,4,2,64]{0,3,2,1:T(8,128)(2,1)S(1)} %get-tuple-element.325), kind=kOutput, calls=%fused_computation.2.clone.1 | convolution fusion | flops 412084224 | bytes 14311424 | tf_op jit(solution)/shard_map/cond/branch_1_fun/while/body/eval_jaxpr/qhcd,khcd->hcqk/dot_general | solution.py:68
  310.7 6.5 %fusion.73 = f32[4,2,768]{2,1,0:T(2,128)S(1)} fusion(f32[4,2,512,768]{3,2,1,0:T(8,128)} %get-tuple-element.292, f32[4,2,768]{2,1,0:T(2,128)S(1)} %fusion.72, pred[768,512]{0,1:T(8,128)(4,1)S(1)} %broadcast_compare_fusion.2), kind=kLoop, calls=%fused_computation.4.clone.1 | loop fusion | flops 15722496 | bytes 13025280 | tf_op jit(solution)/shard_map/cond/branch_1_fun/while/body/eval_jaxpr/reduce_sum | solution.py:77
  319.9 9.0 %fusion.75 = f32[4,2,768,128]{3,2,1,0:T(8,128)} fusion(f32[4,2,768,128]{3,2,1,0:T(8,128)} %get-tuple-element.310, bf16[512,4,128,1]{0,2,3,1:T(8,128)(2,1)S(1)} %bitcast.93, f32[4,2,512,768]{3,2,1,0:T(8,128)} %get-tuple-element.292, f32[4,2,768]{2,1,0:T(2,128)S(1)} %fusion.72, pred[768,512]{0,1:T(8,128)(4,1)S(1)} %broadcast_compare_fusion.2, ...), kind=kOutput, calls=%fused_computation.8.clone.1 | convolution fusion | flops 823394304 | bytes 19841024 | tf_op jit(solution)/shard_map/cond/branch_1_fun/while/body/eval_jaxpr/hcqk,khe->hcqe/dot_general | solution.py:78
  330.3 6.6 %fusion.71 = (f32[4,2,768]{2,1,0:T(2,128)S(1)}, f32[4,2,512,768]{3,2,1,0:T(8,128)}) fusion(pred[768,512]{0,1:T(8,128)(4,1)S(1)} %broadcast_compare_fusion.2, bf16[512,4,2,64]{0,3,2,1:T(8,128)(2,1)S(1)} %bitcast.92, bf16[768,4,2,64]{0,3,2,1:T(8,128)(2,1)S(1)} %get-tuple-element.325), kind=kOutput, calls=%fused_computation.2.clone.1 | convolution fusion | flops 412084224 | bytes 14311424 | tf_op jit(solution)/shard_map/cond/branch_1_fun/while/body/eval_jaxpr/qhcd,khcd->hcqk/dot_general | solution.py:68
  336.9 6.5 %fusion.73 = f32[4,2,768]{2,1,0:T(2,128)S(1)} fusion(f32[4,2,512,768]{3,2,1,0:T(8,128)} %get-tuple-element.292, f32[4,2,768]{2,1,0:T(2,128)S(1)} %fusion.72, pred[768,512]{0,1:T(8,128)(4,1)S(1)} %broadcast_compare_fusion.2), kind=kLoop, calls=%fused_computation.4.clone.1 | loop fusion | flops 15722496 | bytes 13025280 | tf_op jit(solution)/shard_map/cond/branch_1_fun/while/body/eval_jaxpr/reduce_sum | solution.py:77
  346.1 9.0 %fusion.75 = f32[4,2,768,128]{3,2,1,0:T(8,128)} fusion(f32[4,2,768,128]{3,2,1,0:T(8,128)} %get-tuple-element.310, bf16[512,4,128,1]{0,2,3,1:T(8,128)(2,1)S(1)} %bitcast.93, f32[4,2,512,768]{3,2,1,0:T(8,128)} %get-tuple-element.292, f32[4,2,768]{2,1,0:T(2,128)S(1)} %fusion.72, pred[768,512]{0,1:T(8,128)(4,1)S(1)} %broadcast_compare_fusion.2, ...), kind=kOutput, calls=%fused_computation.8.clone.1 | convolution fusion | flops 823394304 | bytes 19841024 | tf_op jit(solution)/shard_map/cond/branch_1_fun/while/body/eval_jaxpr/hcqk,khe->hcqe/dot_general | solution.py:78
  356.4 6.6 %fusion.71 = (f32[4,2,768]{2,1,0:T(2,128)S(1)}, f32[4,2,512,768]{3,2,1,0:T(8,128)}) fusion(pred[768,512]{0,1:T(8,128)(4,1)S(1)} %broadcast_compare_fusion.2, bf16[512,4,2,64]{0,3,2,1:T(8,128)(2,1)S(1)} %bitcast.92, bf16[768,4,2,64]{0,3,2,1:T(8,128)(2,1)S(1)} %get-tuple-element.325), kind=kOutput, calls=%fused_computation.2.clone.1 | convolution fusion | flops 412084224 | bytes 14311424 | tf_op jit(solution)/shard_map/cond/branch_1_fun/while/body/eval_jaxpr/qhcd,khcd->hcqk/dot_general | solution.py:68
  363.0 6.5 %fusion.73 = f32[4,2,768]{2,1,0:T(2,128)S(1)} fusion(f32[4,2,512,768]{3,2,1,0:T(8,128)} %get-tuple-element.292, f32[4,2,768]{2,1,0:T(2,128)S(1)} %fusion.72, pred[768,512]{0,1:T(8,128)(4,1)S(1)} %broadcast_compare_fusion.2), kind=kLoop, calls=%fused_computation.4.clone.1 | loop fusion | flops 15722496 | bytes 13025280 | tf_op jit(solution)/shard_map/cond/branch_1_fun/while/body/eval_jaxpr/reduce_sum | solution.py:77
  372.2 9.0 %fusion.75 = f32[4,2,768,128]{3,2,1,0:T(8,128)} fusion(f32[4,2,768,128]{3,2,1,0:T(8,128)} %get-tuple-element.310, bf16[512,4,128,1]{0,2,3,1:T(8,128)(2,1)S(1)} %bitcast.93, f32[4,2,512,768]{3,2,1,0:T(8,128)} %get-tuple-element.292, f32[4,2,768]{2,1,0:T(2,128)S(1)} %fusion.72, pred[768,512]{0,1:T(8,128)(4,1)S(1)} %broadcast_compare_fusion.2, ...), kind=kOutput, calls=%fused_computation.8.clone.1 | convolution fusion | flops 823394304 | bytes 19841024 | tf_op jit(solution)/shard_map/cond/branch_1_fun/while/body/eval_jaxpr/hcqk,khe->hcqe/dot_general | solution.py:78
  382.6 6.6 %fusion.71 = (f32[4,2,768]{2,1,0:T(2,128)S(1)}, f32[4,2,512,768]{3,2,1,0:T(8,128)}) fusion(pred[768,512]{0,1:T(8,128)(4,1)S(1)} %broadcast_compare_fusion.2, bf16[512,4,2,64]{0,3,2,1:T(8,128)(2,1)S(1)} %bitcast.92, bf16[768,4,2,64]{0,3,2,1:T(8,128)(2,1)S(1)} %get-tuple-element.325), kind=kOutput, calls=%fused_computation.2.clone.1 | convolution fusion | flops 412084224 | bytes 14311424 | tf_op jit(solution)/shard_map/cond/branch_1_fun/while/body/eval_jaxpr/qhcd,khcd->hcqk/dot_general | solution.py:68
  389.2 6.5 %fusion.73 = f32[4,2,768]{2,1,0:T(2,128)S(1)} fusion(f32[4,2,512,768]{3,2,1,0:T(8,128)} %get-tuple-element.292, f32[4,2,768]{2,1,0:T(2,128)S(1)} %fusion.72, pred[768,512]{0,1:T(8,128)(4,1)S(1)} %broadcast_compare_fusion.2), kind=kLoop, calls=%fused_computation.4.clone.1 | loop fusion | flops 15722496 | bytes 13025280 | tf_op jit(solution)/shard_map/cond/branch_1_fun/while/body/eval_jaxpr/reduce_sum | solution.py:77
  398.3 9.0 %fusion.75 = f32[4,2,768,128]{3,2,1,0:T(8,128)} fusion(f32[4,2,768,128]{3,2,1,0:T(8,128)} %get-tuple-element.310, bf16[512,4,128,1]{0,2,3,1:T(8,128)(2,1)S(1)} %bitcast.93, f32[4,2,512,768]{3,2,1,0:T(8,128)} %get-tuple-element.292, f32[4,2,768]{2,1,0:T(2,128)S(1)} %fusion.72, pred[768,512]{0,1:T(8,128)(4,1)S(1)} %broadcast_compare_fusion.2, ...), kind=kOutput, calls=%fused_computation.8.clone.1 | convolution fusion | flops 823394304 | bytes 19841024 | tf_op jit(solution)/shard_map/cond/branch_1_fun/while/body/eval_jaxpr/hcqk,khe->hcqe/dot_general | solution.py:78
  408.7 6.6 %fusion.71 = (f32[4,2,768]{2,1,0:T(2,128)S(1)}, f32[4,2,512,768]{3,2,1,0:T(8,128)}) fusion(pred[768,512]{0,1:T(8,128)(4,1)S(1)} %broadcast_compare_fusion.2, bf16[512,4,2,64]{0,3,2,1:T(8,128)(2,1)S(1)} %bitcast.92, bf16[768,4,2,64]{0,3,2,1:T(8,128)(2,1)S(1)} %get-tuple-element.325), kind=kOutput, calls=%fused_computation.2.clone.1 | convolution fusion | flops 412084224 | bytes 14311424 | tf_op jit(solution)/shard_map/cond/branch_1_fun/while/body/eval_jaxpr/qhcd,khcd->hcqk/dot_general | solution.py:68
  415.3 6.5 %fusion.73 = f32[4,2,768]{2,1,0:T(2,128)S(1)} fusion(f32[4,2,512,768]{3,2,1,0:T(8,128)} %get-tuple-element.292, f32[4,2,768]{2,1,0:T(2,128)S(1)} %fusion.72, pred[768,512]{0,1:T(8,128)(4,1)S(1)} %broadcast_compare_fusion.2), kind=kLoop, calls=%fused_computation.4.clone.1 | loop fusion | flops 15722496 | bytes 13025280 | tf_op jit(solution)/shard_map/cond/branch_1_fun/while/body/eval_jaxpr/reduce_sum | solution.py:77
  424.5 9.0 %fusion.75 = f32[4,2,768,128]{3,2,1,0:T(8,128)} fusion(f32[4,2,768,128]{3,2,1,0:T(8,128)} %get-tuple-element.310, bf16[512,4,128,1]{0,2,3,1:T(8,128)(2,1)S(1)} %bitcast.93, f32[4,2,512,768]{3,2,1,0:T(8,128)} %get-tuple-element.292, f32[4,2,768]{2,1,0:T(2,128)S(1)} %fusion.72, pred[768,512]{0,1:T(8,128)(4,1)S(1)} %broadcast_compare_fusion.2, ...), kind=kOutput, calls=%fused_computation.8.clone.1 | convolution fusion | flops 823394304 | bytes 19841024 | tf_op jit(solution)/shard_map/cond/branch_1_fun/while/body/eval_jaxpr/hcqk,khe->hcqe/dot_general | solution.py:78
  434.9 6.6 %fusion.71 = (f32[4,2,768]{2,1,0:T(2,128)S(1)}, f32[4,2,512,768]{3,2,1,0:T(8,128)}) fusion(pred[768,512]{0,1:T(8,128)(4,1)S(1)} %broadcast_compare_fusion.2, bf16[512,4,2,64]{0,3,2,1:T(8,128)(2,1)S(1)} %bitcast.92, bf16[768,4,2,64]{0,3,2,1:T(8,128)(2,1)S(1)} %get-tuple-element.325), kind=kOutput, calls=%fused_computation.2.clone.1 | convolution fusion | flops 412084224 | bytes 14311424 | tf_op jit(solution)/shard_map/cond/branch_1_fun/while/body/eval_jaxpr/qhcd,khcd->hcqk/dot_general | solution.py:68
  441.5 6.5 %fusion.73 = f32[4,2,768]{2,1,0:T(2,128)S(1)} fusion(f32[4,2,512,768]{3,2,1,0:T(8,128)} %get-tuple-element.292, f32[4,2,768]{2,1,0:T(2,128)S(1)} %fusion.72, pred[768,512]{0,1:T(8,128)(4,1)S(1)} %broadcast_compare_fusion.2), kind=kLoop, calls=%fused_computation.4.clone.1 | loop fusion | flops 15722496 | bytes 13025280 | tf_op jit(solution)/shard_map/cond/branch_1_fun/while/body/eval_jaxpr/reduce_sum | solution.py:77
  450.6 9.0 %fusion.75 = f32[4,2,768,128]{3,2,1,0:T(8,128)} fusion(f32[4,2,768,128]{3,2,1,0:T(8,128)} %get-tuple-element.310, bf16[512,4,128,1]{0,2,3,1:T(8,128)(2,1)S(1)} %bitcast.93, f32[4,2,512,768]{3,2,1,0:T(8,128)} %get-tuple-element.292, f32[4,2,768]{2,1,0:T(2,128)S(1)} %fusion.72, pred[768,512]{0,1:T(8,128)(4,1)S(1)} %broadcast_compare_fusion.2, ...), kind=kOutput, calls=%fused_computation.8.clone.1 | convolution fusion | flops 823394304 | bytes 19841024 | tf_op jit(solution)/shard_map/cond/branch_1_fun/while/body/eval_jaxpr/hcqk,khe->hcqe/dot_general | solution.py:78
  461.0 6.6 %fusion.71 = (f32[4,2,768]{2,1,0:T(2,128)S(1)}, f32[4,2,512,768]{3,2,1,0:T(8,128)}) fusion(pred[768,512]{0,1:T(8,128)(4,1)S(1)} %broadcast_compare_fusion.2, bf16[512,4,2,64]{0,3,2,1:T(8,128)(2,1)S(1)} %bitcast.92, bf16[768,4,2,64]{0,3,2,1:T(8,128)(2,1)S(1)} %get-tuple-element.325), kind=kOutput, calls=%fused_computation.2.clone.1 | convolution fusion | flops 412084224 | bytes 14311424 | tf_op jit(solution)/shard_map/cond/branch_1_fun/while/body/eval_jaxpr/qhcd,khcd->hcqk/dot_general | solution.py:68
  467.6 6.5 %fusion.73 = f32[4,2,768]{2,1,0:T(2,128)S(1)} fusion(f32[4,2,512,768]{3,2,1,0:T(8,128)} %get-tuple-element.292, f32[4,2,768]{2,1,0:T(2,128)S(1)} %fusion.72, pred[768,512]{0,1:T(8,128)(4,1)S(1)} %broadcast_compare_fusion.2), kind=kLoop, calls=%fused_computation.4.clone.1 | loop fusion | flops 15722496 | bytes 13025280 | tf_op jit(solution)/shard_map/cond/branch_1_fun/while/body/eval_jaxpr/reduce_sum | solution.py:77
  476.8 9.0 %fusion.75 = f32[4,2,768,128]{3,2,1,0:T(8,128)} fusion(f32[4,2,768,128]{3,2,1,0:T(8,128)} %get-tuple-element.310, bf16[512,4,128,1]{0,2,3,1:T(8,128)(2,1)S(1)} %bitcast.93, f32[4,2,512,768]{3,2,1,0:T(8,128)} %get-tuple-element.292, f32[4,2,768]{2,1,0:T(2,128)S(1)} %fusion.72, pred[768,512]{0,1:T(8,128)(4,1)S(1)} %broadcast_compare_fusion.2, ...), kind=kOutput, calls=%fused_computation.8.clone.1 | convolution fusion | flops 823394304 | bytes 19841024 | tf_op jit(solution)/shard_map/cond/branch_1_fun/while/body/eval_jaxpr/hcqk,khe->hcqe/dot_general | solution.py:78
  487.2 6.6 %fusion.71 = (f32[4,2,768]{2,1,0:T(2,128)S(1)}, f32[4,2,512,768]{3,2,1,0:T(8,128)}) fusion(pred[768,512]{0,1:T(8,128)(4,1)S(1)} %broadcast_compare_fusion.2, bf16[512,4,2,64]{0,3,2,1:T(8,128)(2,1)S(1)} %bitcast.92, bf16[768,4,2,64]{0,3,2,1:T(8,128)(2,1)S(1)} %get-tuple-element.325), kind=kOutput, calls=%fused_computation.2.clone.1 | convolution fusion | flops 412084224 | bytes 14311424 | tf_op jit(solution)/shard_map/cond/branch_1_fun/while/body/eval_jaxpr/qhcd,khcd->hcqk/dot_general | solution.py:68
  493.8 6.5 %fusion.73 = f32[4,2,768]{2,1,0:T(2,128)S(1)} fusion(f32[4,2,512,768]{3,2,1,0:T(8,128)} %get-tuple-element.292, f32[4,2,768]{2,1,0:T(2,128)S(1)} %fusion.72, pred[768,512]{0,1:T(8,128)(4,1)S(1)} %broadcast_compare_fusion.2), kind=kLoop, calls=%fused_computation.4.clone.1 | loop fusion | flops 15722496 | bytes 13025280 | tf_op jit(solution)/shard_map/cond/branch_1_fun/while/body/eval_jaxpr/reduce_sum | solution.py:77
  502.9 9.0 %fusion.75 = f32[4,2,768,128]{3,2,1,0:T(8,128)} fusion(f32[4,2,768,128]{3,2,1,0:T(8,128)} %get-tuple-element.310, bf16[512,4,128,1]{0,2,3,1:T(8,128)(2,1)S(1)} %bitcast.93, f32[4,2,512,768]{3,2,1,0:T(8,128)} %get-tuple-element.292, f32[4,2,768]{2,1,0:T(2,128)S(1)} %fusion.72, pred[768,512]{0,1:T(8,128)(4,1)S(1)} %broadcast_compare_fusion.2, ...), kind=kOutput, calls=%fused_computation.8.clone.1 | convolution fusion | flops 823394304 | bytes 19841024 | tf_op jit(solution)/shard_map/cond/branch_1_fun/while/body/eval_jaxpr/hcqk,khe->hcqe/dot_general | solution.py:78
  513.3 6.6 %fusion.71 = (f32[4,2,768]{2,1,0:T(2,128)S(1)}, f32[4,2,512,768]{3,2,1,0:T(8,128)}) fusion(pred[768,512]{0,1:T(8,128)(4,1)S(1)} %broadcast_compare_fusion.2, bf16[512,4,2,64]{0,3,2,1:T(8,128)(2,1)S(1)} %bitcast.92, bf16[768,4,2,64]{0,3,2,1:T(8,128)(2,1)S(1)} %get-tuple-element.325), kind=kOutput, calls=%fused_computation.2.clone.1 | convolution fusion | flops 412084224 | bytes 14311424 | tf_op jit(solution)/shard_map/cond/branch_1_fun/while/body/eval_jaxpr/qhcd,khcd->hcqk/dot_general | solution.py:68
  519.9 6.5 %fusion.73 = f32[4,2,768]{2,1,0:T(2,128)S(1)} fusion(f32[4,2,512,768]{3,2,1,0:T(8,128)} %get-tuple-element.292, f32[4,2,768]{2,1,0:T(2,128)S(1)} %fusion.72, pred[768,512]{0,1:T(8,128)(4,1)S(1)} %broadcast_compare_fusion.2), kind=kLoop, calls=%fused_computation.4.clone.1 | loop fusion | flops 15722496 | bytes 13025280 | tf_op jit(solution)/shard_map/cond/branch_1_fun/while/body/eval_jaxpr/reduce_sum | solution.py:77
  529.1 9.0 %fusion.75 = f32[4,2,768,128]{3,2,1,0:T(8,128)} fusion(f32[4,2,768,128]{3,2,1,0:T(8,128)} %get-tuple-element.310, bf16[512,4,128,1]{0,2,3,1:T(8,128)(2,1)S(1)} %bitcast.93, f32[4,2,512,768]{3,2,1,0:T(8,128)} %get-tuple-element.292, f32[4,2,768]{2,1,0:T(2,128)S(1)} %fusion.72, pred[768,512]{0,1:T(8,128)(4,1)S(1)} %broadcast_compare_fusion.2, ...), kind=kOutput, calls=%fused_computation.8.clone.1 | convolution fusion | flops 823394304 | bytes 19841024 | tf_op jit(solution)/shard_map/cond/branch_1_fun/while/body/eval_jaxpr/hcqk,khe->hcqe/dot_general | solution.py:78
  543.6 8.2 %add_convert_fusion = bf16[768,4096]{1,0:T(8,128)(2,1)} fusion(f32[768,4096]{1,0:T(8,128)} %fusion.33, bf16[768,512]{0,1:T(8,128)(2,1)S(1)} %bitcast.98, bf16[512,4096]{1,0:T(8,128)(2,1)S(1)} %copy-done.6), kind=kOutput, calls=%fused_computation.22 | convolution fusion | flops 3227516928 | bytes 23855104 | tf_op jit(solution)/shard_map/dot_general | solution.py:135
  552.5 55.6 %reduce-scatter.2.cloned.1.call-done = bf16[768,1024]{1,0:T(8,128)(2,1)} async-done(((bf16[768,4096]{1,0:T(8,128)(2,1)}), bf16[768,1024]{1,0:T(8,128)(2,1)}) %reduce-scatter.2.cloned.1.call-update) | async-done | bytes 1572880 | tf_op jit(solution)/shard_map/reduce_scatter | solution.py:138
  610.0 5.9 all-reduce
  (149 shorter events, 76.0 us)
Async XLA Ops:
  6.5 119.5 %all-gather.3.cloned.1.call-start = ((), (), s32[]{:S(2)}) async-start(), calls=%async_computation.1 | async-start | bytes 7077888 | tf_op jit(solution)/shard_map/all_gather | solution.py:92
  6.5 9.9 %copy-start.3 = (bf16[768,4096]{1,0:T(8,128)(2,1)S(1)}, bf16[768,4096]{1,0:T(8,128)(2,1)}, u32[]{:S(2)}) copy-start(bf16[768,4096]{1,0:T(8,128)(2,1)} %param.17) | copy-start | bytes 18874372
  6.6 9.9 %copy-start.4 = (bf16[4096,512]{1,0:T(8,128)(2,1)S(1)}, bf16[4096,512]{1,0:T(8,128)(2,1)}, u32[]{:S(2)}) copy-start(bf16[4096,512]{1,0:T(8,128)(2,1)} %param.23) | copy-start | bytes 12582916
  24.7 200.8 %all-gather.5.cloned.1.call-start = ((), (), s32[]{:S(2)}) async-start(), calls=%async_computation.2 | async-start | bytes 7077888 | tf_op jit(solution)/shard_map/all_gather | solution.py:93
  33.0 575.0 %reduce-scatter.2.cloned.1.call-start = ((), (), s32[]{:S(2)}) async-start(), calls=%async_computation.3 | async-start | bytes 7864320 | tf_op jit(solution)/shard_map/reduce_scatter | solution.py:138
  33.3 8.4 %copy-start.5 = (bf16[4096,512]{1,0:T(8,128)(2,1)S(1)}, bf16[4096,512]{1,0:T(8,128)(2,1)}, u32[]{:S(2)}) copy-start(bf16[4096,512]{1,0:T(8,128)(2,1)} %param.19) | copy-start | bytes 12582916
  41.7 10.2 %copy-start = (bf16[3,512]{1,0:T(4,128)(2,1)S(1)}, bf16[3,512]{1,0:T(4,128)(2,1)}, u32[]{:S(2)}) copy-start(bf16[3,512]{1,0:T(4,128)(2,1)} %param.21) | copy-start | bytes 9220
  41.7 10.2 %copy-start.7 = (bf16[128]{0:T(256)(128)(2,1)S(1)}, bf16[128]{0:T(256)(128)(2,1)}, u32[]{:S(2)}) copy-start(bf16[128]{0:T(256)(128)(2,1)} %param.26) | copy-start | bytes 772
  47.2 4.7 copy-start.2
  47.2 5.9 collective-permute-start
  538.9 2.4 copy-start.1
  541.4 2.2 copy-start.6
Sparse Core Ops, SparseCore 0:
  24.8 101.1 all-gather.2
  128.2 97.2 all-gather.4
  551.9 56.0 reduce-scatter.1
where the time goes:
time: 628 us; the launch traced here: 625 us
  matrix products  243 us (39%)
  waiting for transfers between devices  214 us (34%)
  other arithmetic  110 us (18%)
  local copies, waits for them, and re-layouts  34.1 us (5%)
  between operations  13.4 us (2%)
    dot_general x12, matrix products, attend(): jnp.einsum('hcqk,khe->hcqe', weights.astype(jnp.bfloat16), vals_blk, pref...  107 us
    all_gather x1, waiting for transfers between devices, per_device(): value_piece = lax.all_gather(values, 'sp', axis=0, tiled=True)  99.4 us
    dot_general x12, matrix products, attend(): jnp.einsum('qhcd,khcd->hcqk', query_rot, keys_blk, preferred_element_type...  78.7 us
    reduce_sum x12, other arithmetic, attend(): running_sum = running_sum * factor + jnp.sum(weights, axis=-1)  77.7 us
    all_gather x1, waiting for transfers between devices, per_device(): key_piece = lax.all_gather(packed_keys, 'sp', axis=0, tiled=True)  57.8 us
    reduce_scatter x1, waiting for transfers between devices, per_device(): lax.psum_scatter(partial_value.astype(jnp.bfloat16), 'tp', scatter_dimens...  55.6 us
    dot_general x5, matrix products, project(): jnp.dot(hidden_states, weight, preferred_element_type=jnp.float32)  33.6 us
    add x12, other arithmetic, attend(): running_sum = running_sum * factor + jnp.sum(weights, axis=-1)  16 us
  transfers between devices with their start and end apart: 4, of which 4 were waited for; matrix products, arithmetic and copies ran while one was open for 6% of the time, Pallas kernels for 0%

commit v1 on v0

--- a/solution.py
+++ b/solution.py
@@ -89,8 +89,11 @@
         jnp.zeros((head_count, 2, tok_rows, VD), jnp.float32),
     )
     packed_keys = key_rot.reshape(tok_rows, head_count * 2 * QK)
-    key_piece = lax.all_gather(packed_keys, "sp", axis=0, tiled=True)
-    value_piece = lax.all_gather(values, "sp", axis=0, tiled=True)
+    key_piece, value_piece = jnp.split(
+        lax.all_gather(jnp.concatenate([packed_keys, values], axis=1), "sp", axis=0, tiled=True),
+        [packed_keys.shape[1]],
+        axis=1,
+    )
     count = key_piece.shape[0]
     block = 512
 

time: 628 us -> 593 us (0.944)
  matrix products: 243 us -> 212 us
  waiting for transfers between devices: 214 us -> 201 us
  other arithmetic: 110 us -> 119 us
    dot_general x12, matrix products: 107 us -> 81.2 us  [attend(): jnp.einsum('hcqk,khe->hcqe', weights.astype(jnp.bfloat16), vals_blk, pref...]
    dynamic_slice x12 -> x0, local copies, waits for them, and re-layouts: 12.9 us -> none  [one_block(): lax.dynamic_slice_in_dim(key_piece, first, block, 0)]
    all_gather x2 -> x1, waiting for transfers between devices: 157 us -> 145 us  [per_device(): lax.all_gather(jnp.concatenate([packed_keys, values], axis=1), 'sp', axis...]
    split x0 -> x1, local copies, waits for them, and re-layouts: none -> 10.6 us  [per_device(): jnp.split(lax.all_gather(jnp.concatenate([packed_keys, values], axis=1),...]
    dynamic_slice x24 -> x12, local copies, waits for them, and re-layouts: 15.5 us -> 15.3 us  [one_block(): lax.dynamic_slice_in_dim(value_piece, first, block, 0)]
  transfers between devices with their start and end apart: 4 -> 3, of which waited for: 4 -> 3; matrix products, arithmetic and copies ran while one was open for 6% -> 5% of each run, Pallas kernels for 0% -> 0%
where the time goes in v1:
time: 593 us; the launch traced here: 592 us
  matrix products  212 us (36%)
  waiting for transfers between devices  201 us (34%)
  other arithmetic  119 us (20%)
  local copies, waits for them, and re-layouts  34 us (6%)
  between operations  13.7 us (2%)
    all_gather x1, waiting for transfers between devices, per_device(): lax.all_gather(jnp.concatenate([packed_keys, values], axis=1), 'sp', axis...  145 us
    reduce_sum x12, other arithmetic, attend(): running_sum = running_sum * factor + jnp.sum(weights, axis=-1)  81.2 us
    dot_general x12, matrix products, attend(): jnp.einsum('hcqk,khe->hcqe', weights.astype(jnp.bfloat16), vals_blk, pref...  81.2 us
    dot_general x12, matrix products, attend(): jnp.einsum('qhcd,khcd->hcqk', query_rot, keys_blk, preferred_element_type...  80.2 us
    reduce_scatter x1, waiting for transfers between devices, per_device(): lax.psum_scatter(partial_value.astype(jnp.bfloat16), 'tp', scatter_dimens...  55.5 us
    dot_general x5, matrix products, project(): jnp.dot(hidden_states, weight, preferred_element_type=jnp.float32)  28.2 us
    add x12, other arithmetic, attend(): running_sum = running_sum * factor + jnp.sum(weights, axis=-1)  21.4 us
    dynamic_slice x12, local copies, waits for them, and re-layouts, one_block(): lax.dynamic_slice_in_dim(value_piece, first, block, 0)  15.3 us
  transfers between devices with their start and end apart: 3, of which 3 were waited for; matrix products, arithmetic and copies ran while one was open for 5% of the time, Pallas kernels for 0%

profile of v1, /device:TPU:0, one launch (start us, length us, event | category | flops | bytes accessed | tf_op | source)
XLA Modules:
  0.0 592.1 jit_solution(9650800619546742597)
XLA Ops:
  6.6 7.6 %convolution_convert_fusion = bf16[768,512]{0,1:T(8,128)(2,1)S(1)} fusion(bf16[768,4096]{1,0:T(8,128)(2,1)} %param.17, bf16[4096,512]{1,0:T(8,128)(2,1)} %param.22), kind=kOutput, calls=%fused_computation.57 | convolution fusion | flops 3221618688 | bytes 11272192 | tf_op jit(solution)/shard_map/dot_general | solution.py:52
  30.8 7.6 %convolution_convert_fusion.3 = bf16[768,512]{1,0:T(8,128)(2,1)S(1)} fusion(bf16[768,4096]{1,0:T(8,128)(2,1)} %param.17, bf16[4096,512]{1,0:T(8,128)(2,1)} %param.20), kind=kOutput, calls=%fused_computation.61 | convolution fusion | flops 3221618688 | bytes 11272192 | tf_op jit(solution)/shard_map/dot_general | solution.py:52
  38.4 5.5 convert_multiply_fusion.1
  43.9 5.3 collective-permute-start
  50.5 14.2 %fusion.33 = f32[768,4096]{1,0:T(8,128)} fusion(bf16[512,4096]{1,0:T(8,128)(2,1)} %param.27, f32[2,512]{1,0:T(2,128)S(1)} %collective-permute-done, f32[768,512]{1,0:T(8,128)S(1)} %convert_multiply_fusion.1, bf16[768,4096]{1,0:T(8,128)(2,1)} %param.17, bf16[4096,512]{1,0:T(8,128)(2,1)} %param.18, f32[512]{0:T(512)S(1)} %bitcast.103, f32[512]{0:T(512)S(1)} %bitcast.102, ...), kind=kOutput, calls=%fused_computation.66 | convolution fusion | flops 6446776320 | bytes 28846080 | tf_op jit(solution)/shard_map/dot_general | solution.py:138
  64.7 144.5 %all-gather.2.cloned.1.call-done = bf16[6144,1024]{0,1:T(8,128)(2,1)} async-done(((bf16[768,1024]{0,1:T(8,128)(2,1)}), bf16[6144,1024]{0,1:T(8,128)(2,1)}) %all-gather.2.cloned.1.call-update) | async-done | bytes 12582928 | tf_op jit(solution)/shard_map/all_gather | solution.py:93
  209.3 295.2 %conditional.1 = (f32[4,2,768]{2,1,0:T(2,128)}, f32[4,2,768,128]{3,2,1,0:T(8,128)}) conditional(s32[]{:T(128)} %convert_element_type.98, () %tuple.27, (bf16[6144,1024]{0,1:T(8,128)(2,1)}, s32[]{:T(128)}, s32[768]{0:T(1024)S(1)}, bf16[768,4,2,64]{0,3,2,1:T(8,128)(2,1)S(1)}) %tuple.28), branch_computations={%region_0.0_spmd, %region_1.6_spmd} | conditional | flops 1251638528 | bytes 125449552 | solution.py:113
  209.3 10.6 %fusion.38 = (bf16[6144,512]{0,1:T(8,128)(2,1)}, bf16[6144,512]{0,1:T(8,128)(2,1)}) fusion(bf16[6144,1024]{0,1:T(8,128)(2,1)} %get-tuple-element.158), kind=kLoop, calls=%fused_computation.80 | loop fusion | bytes 25165824 | tf_op jit(solution)/shard_map/split | solution.py:92
  219.9 284.6 %while.17 = (s32[]{:T(128)}, f32[4,2,768]{2,1,0:T(2,128)S(1)}, f32[4,2,768]{2,1,0:T(2,128)}, f32[4,2,768,128]{3,2,1,0:T(8,128)}, s32[768]{0:T(1024)S(1)}, /*inde...) while((s32[]{:T(128)}, f32[4,2,768]{2,1,0:T(2,128)S(1)}, ...), condition=%wide.region_5.5_spmd.clone, body=%wide.region_2.4_spmd.clone.sunk | while | flops 1251637760 | bytes 100277456 | solution.py:111
  221.5 6.7 %fusion.72 = (f32[4,2,768]{2,1,0:T(2,128)S(1)}, f32[4,2,512,768]{3,2,1,0:T(8,128)}) fusion(pred[768,512]{0,1:T(8,128)(4,1)S(1)} %broadcast_compare_fusion.2, bf16[512,4,2,64]{0,3,2,1:T(8,128)(2,1)S(1)} %bitcast.92, bf16[768,4,2,64]{0,3,2,1:T(8,128)(2,1)S(1)} %get-tuple-element.332), kind=kOutput, calls=%fused_computation.2.clone.1 | convolution fusion | flops 412084224 | bytes 14311424 | tf_op jit(solution)/shard_map/cond/branch_1_fun/while/body/eval_jaxpr/qhcd,khcd->hcqk/dot_general | solution.py:68
  228.2 6.8 %fusion.74 = f32[4,2,768]{2,1,0:T(2,128)S(1)} fusion(f32[4,2,512,768]{3,2,1,0:T(8,128)} %get-tuple-element.298, f32[4,2,768]{2,1,0:T(2,128)S(1)} %fusion.73, pred[768,512]{0,1:T(8,128)(4,1)S(1)} %broadcast_compare_fusion.2), kind=kLoop, calls=%fused_computation.4.clone.1 | loop fusion | flops 15722496 | bytes 13025280 | tf_op jit(solution)/shard_map/cond/branch_1_fun/while/body/eval_jaxpr/reduce_sum | solution.py:77
  236.5 5.6 fusion.76
  243.7 6.7 %fusion.72 = (f32[4,2,768]{2,1,0:T(2,128)S(1)}, f32[4,2,512,768]{3,2,1,0:T(8,128)}) fusion(pred[768,512]{0,1:T(8,128)(4,1)S(1)} %broadcast_compare_fusion.2, bf16[512,4,2,64]{0,3,2,1:T(8,128)(2,1)S(1)} %bitcast.92, bf16[768,4,2,64]{0,3,2,1:T(8,128)(2,1)S(1)} %get-tuple-element.332), kind=kOutput, calls=%fused_computation.2.clone.1 | convolution fusion | flops 412084224 | bytes 14311424 | tf_op jit(solution)/shard_map/cond/branch_1_fun/while/body/eval_jaxpr/qhcd,khcd->hcqk/dot_general | solution.py:68
  250.5 6.8 %fusion.74 = f32[4,2,768]{2,1,0:T(2,128)S(1)} fusion(f32[4,2,512,768]{3,2,1,0:T(8,128)} %get-tuple-element.298, f32[4,2,768]{2,1,0:T(2,128)S(1)} %fusion.73, pred[768,512]{0,1:T(8,128)(4,1)S(1)} %broadcast_compare_fusion.2), kind=kLoop, calls=%fused_computation.4.clone.1 | loop fusion | flops 15722496 | bytes 13025280 | tf_op jit(solution)/shard_map/cond/branch_1_fun/while/body/eval_jaxpr/reduce_sum | solution.py:77
  259.1 6.9 %fusion.76 = f32[4,2,768,128]{3,2,1,0:T(8,128)} fusion(f32[4,2,768,128]{3,2,1,0:T(8,128)} %get-tuple-element.317, bf16[512,4,128,1]{0,2,3,1:T(8,128)(2,1)S(1)} %bitcast.93, f32[4,2,512,768]{3,2,1,0:T(8,128)S(1)} %copy-done, f32[4,2,768]{2,1,0:T(2,128)S(1)} %fusion.73, pred[768,512]{0,1:T(8,128)(4,1)S(1)} %broadcast_compare_fusion.2, ...), kind=kOutput, calls=%fused_computation.8.clone.1 | convolution fusion | flops 823394304 | bytes 19841024 | tf_op jit(solution)/shard_map/cond/branch_1_fun/while/body/eval_jaxpr/hcqk,khe->hcqe/dot_general | solution.py:78
  267.6 6.7 %fusion.72 = (f32[4,2,768]{2,1,0:T(2,128)S(1)}, f32[4,2,512,768]{3,2,1,0:T(8,128)}) fusion(pred[768,512]{0,1:T(8,128)(4,1)S(1)} %broadcast_compare_fusion.2, bf16[512,4,2,64]{0,3,2,1:T(8,128)(2,1)S(1)} %bitcast.92, bf16[768,4,2,64]{0,3,2,1:T(8,128)(2,1)S(1)} %get-tuple-element.332), kind=kOutput, calls=%fused_computation.2.clone.1 | convolution fusion | flops 412084224 | bytes 14311424 | tf_op jit(solution)/shard_map/cond/branch_1_fun/while/body/eval_jaxpr/qhcd,khcd->hcqk/dot_general | solution.py:68
  274.3 6.8 %fusion.74 = f32[4,2,768]{2,1,0:T(2,128)S(1)} fusion(f32[4,2,512,768]{3,2,1,0:T(8,128)} %get-tuple-element.298, f32[4,2,768]{2,1,0:T(2,128)S(1)} %fusion.73, pred[768,512]{0,1:T(8,128)(4,1)S(1)} %broadcast_compare_fusion.2), kind=kLoop, calls=%fused_computation.4.clone.1 | loop fusion | flops 15722496 | bytes 13025280 | tf_op jit(solution)/shard_map/cond/branch_1_fun/while/body/eval_jaxpr/reduce_sum | solution.py:77
  283.0 6.9 %fusion.76 = f32[4,2,768,128]{3,2,1,0:T(8,128)} fusion(f32[4,2,768,128]{3,2,1,0:T(8,128)} %get-tuple-element.317, bf16[512,4,128,1]{0,2,3,1:T(8,128)(2,1)S(1)} %bitcast.93, f32[4,2,512,768]{3,2,1,0:T(8,128)S(1)} %copy-done, f32[4,2,768]{2,1,0:T(2,128)S(1)} %fusion.73, pred[768,512]{0,1:T(8,128)(4,1)S(1)} %broadcast_compare_fusion.2, ...), kind=kOutput, calls=%fused_computation.8.clone.1 | convolution fusion | flops 823394304 | bytes 19841024 | tf_op jit(solution)/shard_map/cond/branch_1_fun/while/body/eval_jaxpr/hcqk,khe->hcqe/dot_general | solution.py:78
  291.5 6.7 %fusion.72 = (f32[4,2,768]{2,1,0:T(2,128)S(1)}, f32[4,2,512,768]{3,2,1,0:T(8,128)}) fusion(pred[768,512]{0,1:T(8,128)(4,1)S(1)} %broadcast_compare_fusion.2, bf16[512,4,2,64]{0,3,2,1:T(8,128)(2,1)S(1)} %bitcast.92, bf16[768,4,2,64]{0,3,2,1:T(8,128)(2,1)S(1)} %get-tuple-element.332), kind=kOutput, calls=%fused_computation.2.clone.1 | convolution fusion | flops 412084224 | bytes 14311424 | tf_op jit(solution)/shard_map/cond/branch_1_fun/while/body/eval_jaxpr/qhcd,khcd->hcqk/dot_general | solution.py:68
  298.2 6.8 %fusion.74 = f32[4,2,768]{2,1,0:T(2,128)S(1)} fusion(f32[4,2,512,768]{3,2,1,0:T(8,128)} %get-tuple-element.298, f32[4,2,768]{2,1,0:T(2,128)S(1)} %fusion.73, pred[768,512]{0,1:T(8,128)(4,1)S(1)} %broadcast_compare_fusion.2), kind=kLoop, calls=%fused_computation.4.clone.1 | loop fusion | flops 15722496 | bytes 13025280 | tf_op jit(solution)/shard_map/cond/branch_1_fun/while/body/eval_jaxpr/reduce_sum | solution.py:77
  306.8 6.9 %fusion.76 = f32[4,2,768,128]{3,2,1,0:T(8,128)} fusion(f32[4,2,768,128]{3,2,1,0:T(8,128)} %get-tuple-element.317, bf16[512,4,128,1]{0,2,3,1:T(8,128)(2,1)S(1)} %bitcast.93, f32[4,2,512,768]{3,2,1,0:T(8,128)S(1)} %copy-done, f32[4,2,768]{2,1,0:T(2,128)S(1)} %fusion.73, pred[768,512]{0,1:T(8,128)(4,1)S(1)} %broadcast_compare_fusion.2, ...), kind=kOutput, calls=%fused_computation.8.clone.1 | convolution fusion | flops 823394304 | bytes 19841024 | tf_op jit(solution)/shard_map/cond/branch_1_fun/while/body/eval_jaxpr/hcqk,khe->hcqe/dot_general | solution.py:78
  315.3 6.7 %fusion.72 = (f32[4,2,768]{2,1,0:T(2,128)S(1)}, f32[4,2,512,768]{3,2,1,0:T(8,128)}) fusion(pred[768,512]{0,1:T(8,128)(4,1)S(1)} %broadcast_compare_fusion.2, bf16[512,4,2,64]{0,3,2,1:T(8,128)(2,1)S(1)} %bitcast.92, bf16[768,4,2,64]{0,3,2,1:T(8,128)(2,1)S(1)} %get-tuple-element.332), kind=kOutput, calls=%fused_computation.2.clone.1 | convolution fusion | flops 412084224 | bytes 14311424 | tf_op jit(solution)/shard_map/cond/branch_1_fun/while/body/eval_jaxpr/qhcd,khcd->hcqk/dot_general | solution.py:68
  322.0 6.8 %fusion.74 = f32[4,2,768]{2,1,0:T(2,128)S(1)} fusion(f32[4,2,512,768]{3,2,1,0:T(8,128)} %get-tuple-element.298, f32[4,2,768]{2,1,0:T(2,128)S(1)} %fusion.73, pred[768,512]{0,1:T(8,128)(4,1)S(1)} %broadcast_compare_fusion.2), kind=kLoop, calls=%fused_computation.4.clone.1 | loop fusion | flops 15722496 | bytes 13025280 | tf_op jit(solution)/shard_map/cond/branch_1_fun/while/body/eval_jaxpr/reduce_sum | solution.py:77
  330.7 6.9 %fusion.76 = f32[4,2,768,128]{3,2,1,0:T(8,128)} fusion(f32[4,2,768,128]{3,2,1,0:T(8,128)} %get-tuple-element.317, bf16[512,4,128,1]{0,2,3,1:T(8,128)(2,1)S(1)} %bitcast.93, f32[4,2,512,768]{3,2,1,0:T(8,128)S(1)} %copy-done, f32[4,2,768]{2,1,0:T(2,128)S(1)} %fusion.73, pred[768,512]{0,1:T(8,128)(4,1)S(1)} %broadcast_compare_fusion.2, ...), kind=kOutput, calls=%fused_computation.8.clone.1 | convolution fusion | flops 823394304 | bytes 19841024 | tf_op jit(solution)/shard_map/cond/branch_1_fun/while/body/eval_jaxpr/hcqk,khe->hcqe/dot_general | solution.py:78
  339.1 6.7 %fusion.72 = (f32[4,2,768]{2,1,0:T(2,128)S(1)}, f32[4,2,512,768]{3,2,1,0:T(8,128)}) fusion(pred[768,512]{0,1:T(8,128)(4,1)S(1)} %broadcast_compare_fusion.2, bf16[512,4,2,64]{0,3,2,1:T(8,128)(2,1)S(1)} %bitcast.92, bf16[768,4,2,64]{0,3,2,1:T(8,128)(2,1)S(1)} %get-tuple-element.332), kind=kOutput, calls=%fused_computation.2.clone.1 | convolution fusion | flops 412084224 | bytes 14311424 | tf_op jit(solution)/shard_map/cond/branch_1_fun/while/body/eval_jaxpr/qhcd,khcd->hcqk/dot_general | solution.py:68
  345.9 6.8 %fusion.74 = f32[4,2,768]{2,1,0:T(2,128)S(1)} fusion(f32[4,2,512,768]{3,2,1,0:T(8,128)} %get-tuple-element.298, f32[4,2,768]{2,1,0:T(2,128)S(1)} %fusion.73, pred[768,512]{0,1:T(8,128)(4,1)S(1)} %broadcast_compare_fusion.2), kind=kLoop, calls=%fused_computation.4.clone.1 | loop fusion | flops 15722496 | bytes 13025280 | tf_op jit(solution)/shard_map/cond/branch_1_fun/while/body/eval_jaxpr/reduce_sum | solution.py:77
  354.5 6.9 %fusion.76 = f32[4,2,768,128]{3,2,1,0:T(8,128)} fusion(f32[4,2,768,128]{3,2,1,0:T(8,128)} %get-tuple-element.317, bf16[512,4,128,1]{0,2,3,1:T(8,128)(2,1)S(1)} %bitcast.93, f32[4,2,512,768]{3,2,1,0:T(8,128)S(1)} %copy-done, f32[4,2,768]{2,1,0:T(2,128)S(1)} %fusion.73, pred[768,512]{0,1:T(8,128)(4,1)S(1)} %broadcast_compare_fusion.2, ...), kind=kOutput, calls=%fused_computation.8.clone.1 | convolution fusion | flops 823394304 | bytes 19841024 | tf_op jit(solution)/shard_map/cond/branch_1_fun/while/body/eval_jaxpr/hcqk,khe->hcqe/dot_general | solution.py:78
  363.0 6.7 %fusion.72 = (f32[4,2,768]{2,1,0:T(2,128)S(1)}, f32[4,2,512,768]{3,2,1,0:T(8,128)}) fusion(pred[768,512]{0,1:T(8,128)(4,1)S(1)} %broadcast_compare_fusion.2, bf16[512,4,2,64]{0,3,2,1:T(8,128)(2,1)S(1)} %bitcast.92, bf16[768,4,2,64]{0,3,2,1:T(8,128)(2,1)S(1)} %get-tuple-element.332), kind=kOutput, calls=%fused_computation.2.clone.1 | convolution fusion | flops 412084224 | bytes 14311424 | tf_op jit(solution)/shard_map/cond/branch_1_fun/while/body/eval_jaxpr/qhcd,khcd->hcqk/dot_general | solution.py:68
  369.7 6.8 %fusion.74 = f32[4,2,768]{2,1,0:T(2,128)S(1)} fusion(f32[4,2,512,768]{3,2,1,0:T(8,128)} %get-tuple-element.298, f32[4,2,768]{2,1,0:T(2,128)S(1)} %fusion.73, pred[768,512]{0,1:T(8,128)(4,1)S(1)} %broadcast_compare_fusion.2), kind=kLoop, calls=%fused_computation.4.clone.1 | loop fusion | flops 15722496 | bytes 13025280 | tf_op jit(solution)/shard_map/cond/branch_1_fun/while/body/eval_jaxpr/reduce_sum | solution.py:77
  378.4 6.9 %fusion.76 = f32[4,2,768,128]{3,2,1,0:T(8,128)} fusion(f32[4,2,768,128]{3,2,1,0:T(8,128)} %get-tuple-element.317, bf16[512,4,128,1]{0,2,3,1:T(8,128)(2,1)S(1)} %bitcast.93, f32[4,2,512,768]{3,2,1,0:T(8,128)S(1)} %copy-done, f32[4,2,768]{2,1,0:T(2,128)S(1)} %fusion.73, pred[768,512]{0,1:T(8,128)(4,1)S(1)} %broadcast_compare_fusion.2, ...), kind=kOutput, calls=%fused_computation.8.clone.1 | convolution fusion | flops 823394304 | bytes 19841024 | tf_op jit(solution)/shard_map/cond/branch_1_fun/while/body/eval_jaxpr/hcqk,khe->hcqe/dot_general | solution.py:78
  386.8 6.7 %fusion.72 = (f32[4,2,768]{2,1,0:T(2,128)S(1)}, f32[4,2,512,768]{3,2,1,0:T(8,128)}) fusion(pred[768,512]{0,1:T(8,128)(4,1)S(1)} %broadcast_compare_fusion.2, bf16[512,4,2,64]{0,3,2,1:T(8,128)(2,1)S(1)} %bitcast.92, bf16[768,4,2,64]{0,3,2,1:T(8,128)(2,1)S(1)} %get-tuple-element.332), kind=kOutput, calls=%fused_computation.2.clone.1 | convolution fusion | flops 412084224 | bytes 14311424 | tf_op jit(solution)/shard_map/cond/branch_1_fun/while/body/eval_jaxpr/qhcd,khcd->hcqk/dot_general | solution.py:68
  393.6 6.8 %fusion.74 = f32[4,2,768]{2,1,0:T(2,128)S(1)} fusion(f32[4,2,512,768]{3,2,1,0:T(8,128)} %get-tuple-element.298, f32[4,2,768]{2,1,0:T(2,128)S(1)} %fusion.73, pred[768,512]{0,1:T(8,128)(4,1)S(1)} %broadcast_compare_fusion.2), kind=kLoop, calls=%fused_computation.4.clone.1 | loop fusion | flops 15722496 | bytes 13025280 | tf_op jit(solution)/shard_map/cond/branch_1_fun/while/body/eval_jaxpr/reduce_sum | solution.py:77
  402.2 6.9 %fusion.76 = f32[4,2,768,128]{3,2,1,0:T(8,128)} fusion(f32[4,2,768,128]{3,2,1,0:T(8,128)} %get-tuple-element.317, bf16[512,4,128,1]{0,2,3,1:T(8,128)(2,1)S(1)} %bitcast.93, f32[4,2,512,768]{3,2,1,0:T(8,128)S(1)} %copy-done, f32[4,2,768]{2,1,0:T(2,128)S(1)} %fusion.73, pred[768,512]{0,1:T(8,128)(4,1)S(1)} %broadcast_compare_fusion.2, ...), kind=kOutput, calls=%fused_computation.8.clone.1 | convolution fusion | flops 823394304 | bytes 19841024 | tf_op jit(solution)/shard_map/cond/branch_1_fun/while/body/eval_jaxpr/hcqk,khe->hcqe/dot_general | solution.py:78
  410.7 6.7 %fusion.72 = (f32[4,2,768]{2,1,0:T(2,128)S(1)}, f32[4,2,512,768]{3,2,1,0:T(8,128)}) fusion(pred[768,512]{0,1:T(8,128)(4,1)S(1)} %broadcast_compare_fusion.2, bf16[512,4,2,64]{0,3,2,1:T(8,128)(2,1)S(1)} %bitcast.92, bf16[768,4,2,64]{0,3,2,1:T(8,128)(2,1)S(1)} %get-tuple-element.332), kind=kOutput, calls=%fused_computation.2.clone.1 | convolution fusion | flops 412084224 | bytes 14311424 | tf_op jit(solution)/shard_map/cond/branch_1_fun/while/body/eval_jaxpr/qhcd,khcd->hcqk/dot_general | solution.py:68
  417.4 6.8 %fusion.74 = f32[4,2,768]{2,1,0:T(2,128)S(1)} fusion(f32[4,2,512,768]{3,2,1,0:T(8,128)} %get-tuple-element.298, f32[4,2,768]{2,1,0:T(2,128)S(1)} %fusion.73, pred[768,512]{0,1:T(8,128)(4,1)S(1)} %broadcast_compare_fusion.2), kind=kLoop, calls=%fused_computation.4.clone.1 | loop fusion | flops 15722496 | bytes 13025280 | tf_op jit(solution)/shard_map/cond/branch_1_fun/while/body/eval_jaxpr/reduce_sum | solution.py:77
  426.1 6.9 %fusion.76 = f32[4,2,768,128]{3,2,1,0:T(8,128)} fusion(f32[4,2,768,128]{3,2,1,0:T(8,128)} %get-tuple-element.317, bf16[512,4,128,1]{0,2,3,1:T(8,128)(2,1)S(1)} %bitcast.93, f32[4,2,512,768]{3,2,1,0:T(8,128)S(1)} %copy-done, f32[4,2,768]{2,1,0:T(2,128)S(1)} %fusion.73, pred[768,512]{0,1:T(8,128)(4,1)S(1)} %broadcast_compare_fusion.2, ...), kind=kOutput, calls=%fused_computation.8.clone.1 | convolution fusion | flops 823394304 | bytes 19841024 | tf_op jit(solution)/shard_map/cond/branch_1_fun/while/body/eval_jaxpr/hcqk,khe->hcqe/dot_general | solution.py:78
  434.5 6.7 %fusion.72 = (f32[4,2,768]{2,1,0:T(2,128)S(1)}, f32[4,2,512,768]{3,2,1,0:T(8,128)}) fusion(pred[768,512]{0,1:T(8,128)(4,1)S(1)} %broadcast_compare_fusion.2, bf16[512,4,2,64]{0,3,2,1:T(8,128)(2,1)S(1)} %bitcast.92, bf16[768,4,2,64]{0,3,2,1:T(8,128)(2,1)S(1)} %get-tuple-element.332), kind=kOutput, calls=%fused_computation.2.clone.1 | convolution fusion | flops 412084224 | bytes 14311424 | tf_op jit(solution)/shard_map/cond/branch_1_fun/while/body/eval_jaxpr/qhcd,khcd->hcqk/dot_general | solution.py:68
  441.2 6.8 %fusion.74 = f32[4,2,768]{2,1,0:T(2,128)S(1)} fusion(f32[4,2,512,768]{3,2,1,0:T(8,128)} %get-tuple-element.298, f32[4,2,768]{2,1,0:T(2,128)S(1)} %fusion.73, pred[768,512]{0,1:T(8,128)(4,1)S(1)} %broadcast_compare_fusion.2), kind=kLoop, calls=%fused_computation.4.clone.1 | loop fusion | flops 15722496 | bytes 13025280 | tf_op jit(solution)/shard_map/cond/branch_1_fun/while/body/eval_jaxpr/reduce_sum | solution.py:77
  449.9 6.9 %fusion.76 = f32[4,2,768,128]{3,2,1,0:T(8,128)} fusion(f32[4,2,768,128]{3,2,1,0:T(8,128)} %get-tuple-element.317, bf16[512,4,128,1]{0,2,3,1:T(8,128)(2,1)S(1)} %bitcast.93, f32[4,2,512,768]{3,2,1,0:T(8,128)S(1)} %copy-done, f32[4,2,768]{2,1,0:T(2,128)S(1)} %fusion.73, pred[768,512]{0,1:T(8,128)(4,1)S(1)} %broadcast_compare_fusion.2, ...), kind=kOutput, calls=%fused_computation.8.clone.1 | convolution fusion | flops 823394304 | bytes 19841024 | tf_op jit(solution)/shard_map/cond/branch_1_fun/while/body/eval_jaxpr/hcqk,khe->hcqe/dot_general | solution.py:78
  458.4 6.7 %fusion.72 = (f32[4,2,768]{2,1,0:T(2,128)S(1)}, f32[4,2,512,768]{3,2,1,0:T(8,128)}) fusion(pred[768,512]{0,1:T(8,128)(4,1)S(1)} %broadcast_compare_fusion.2, bf16[512,4,2,64]{0,3,2,1:T(8,128)(2,1)S(1)} %bitcast.92, bf16[768,4,2,64]{0,3,2,1:T(8,128)(2,1)S(1)} %get-tuple-element.332), kind=kOutput, calls=%fused_computation.2.clone.1 | convolution fusion | flops 412084224 | bytes 14311424 | tf_op jit(solution)/shard_map/cond/branch_1_fun/while/body/eval_jaxpr/qhcd,khcd->hcqk/dot_general | solution.py:68
  465.1 6.8 %fusion.74 = f32[4,2,768]{2,1,0:T(2,128)S(1)} fusion(f32[4,2,512,768]{3,2,1,0:T(8,128)} %get-tuple-element.298, f32[4,2,768]{2,1,0:T(2,128)S(1)} %fusion.73, pred[768,512]{0,1:T(8,128)(4,1)S(1)} %broadcast_compare_fusion.2), kind=kLoop, calls=%fused_computation.4.clone.1 | loop fusion | flops 15722496 | bytes 13025280 | tf_op jit(solution)/shard_map/cond/branch_1_fun/while/body/eval_jaxpr/reduce_sum | solution.py:77
  473.7 6.9 %fusion.76 = f32[4,2,768,128]{3,2,1,0:T(8,128)} fusion(f32[4,2,768,128]{3,2,1,0:T(8,128)} %get-tuple-element.317, bf16[512,4,128,1]{0,2,3,1:T(8,128)(2,1)S(1)} %bitcast.93, f32[4,2,512,768]{3,2,1,0:T(8,128)S(1)} %copy-done, f32[4,2,768]{2,1,0:T(2,128)S(1)} %fusion.73, pred[768,512]{0,1:T(8,128)(4,1)S(1)} %broadcast_compare_fusion.2, ...), kind=kOutput, calls=%fused_computation.8.clone.1 | convolution fusion | flops 823394304 | bytes 19841024 | tf_op jit(solution)/shard_map/cond/branch_1_fun/while/body/eval_jaxpr/hcqk,khe->hcqe/dot_general | solution.py:78
  482.2 6.7 %fusion.72 = (f32[4,2,768]{2,1,0:T(2,128)S(1)}, f32[4,2,512,768]{3,2,1,0:T(8,128)}) fusion(pred[768,512]{0,1:T(8,128)(4,1)S(1)} %broadcast_compare_fusion.2, bf16[512,4,2,64]{0,3,2,1:T(8,128)(2,1)S(1)} %bitcast.92, bf16[768,4,2,64]{0,3,2,1:T(8,128)(2,1)S(1)} %get-tuple-element.332), kind=kOutput, calls=%fused_computation.2.clone.1 | convolution fusion | flops 412084224 | bytes 14311424 | tf_op jit(solution)/shard_map/cond/branch_1_fun/while/body/eval_jaxpr/qhcd,khcd->hcqk/dot_general | solution.py:68
  488.9 6.8 %fusion.74 = f32[4,2,768]{2,1,0:T(2,128)S(1)} fusion(f32[4,2,512,768]{3,2,1,0:T(8,128)} %get-tuple-element.298, f32[4,2,768]{2,1,0:T(2,128)S(1)} %fusion.73, pred[768,512]{0,1:T(8,128)(4,1)S(1)} %broadcast_compare_fusion.2), kind=kLoop, calls=%fused_computation.4.clone.1 | loop fusion | flops 15722496 | bytes 13025280 | tf_op jit(solution)/shard_map/cond/branch_1_fun/while/body/eval_jaxpr/reduce_sum | solution.py:77
  497.6 6.9 %fusion.76 = f32[4,2,768,128]{3,2,1,0:T(8,128)} fusion(f32[4,2,768,128]{3,2,1,0:T(8,128)} %get-tuple-element.317, bf16[512,4,128,1]{0,2,3,1:T(8,128)(2,1)S(1)} %bitcast.93, f32[4,2,512,768]{3,2,1,0:T(8,128)S(1)} %copy-done, f32[4,2,768]{2,1,0:T(2,128)S(1)} %fusion.73, pred[768,512]{0,1:T(8,128)(4,1)S(1)} %broadcast_compare_fusion.2, ...), kind=kOutput, calls=%fused_computation.8.clone.1 | convolution fusion | flops 823394304 | bytes 19841024 | tf_op jit(solution)/shard_map/cond/branch_1_fun/while/body/eval_jaxpr/hcqk,khe->hcqe/dot_general | solution.py:78
  509.9 8.2 %add_convert_fusion = bf16[768,4096]{1,0:T(8,128)(2,1)} fusion(f32[768,4096]{1,0:T(8,128)} %fusion.33, bf16[768,512]{0,1:T(8,128)(2,1)S(1)} %bitcast.98, bf16[512,4096]{1,0:T(8,128)(2,1)S(1)} %copy-done.7), kind=kOutput, calls=%fused_computation.22 | convolution fusion | flops 3227516928 | bytes 23855104 | tf_op jit(solution)/shard_map/dot_general | solution.py:138
  518.9 55.5 %reduce-scatter.2.cloned.1.call-done = bf16[768,1024]{1,0:T(8,128)(2,1)} async-done(((bf16[768,4096]{1,0:T(8,128)(2,1)}), bf16[768,1024]{1,0:T(8,128)(2,1)}) %reduce-scatter.2.cloned.1.call-update) | async-done | bytes 1572880 | tf_op jit(solution)/shard_map/reduce_scatter | solution.py:141
  576.3 5.9 all-reduce
  (153 shorter events, 70.3 us)
Async XLA Ops:
  6.5 202.7 %all-gather.2.cloned.1.call-start = ((), (), s32[]{:S(2)}) async-start(), calls=%async_computation.1 | async-start | bytes 14155776 | tf_op jit(solution)/shard_map/all_gather | solution.py:93
  6.5 9.9 %copy-start.3 = (bf16[768,4096]{1,0:T(8,128)(2,1)S(1)}, bf16[768,4096]{1,0:T(8,128)(2,1)}, u32[]{:S(2)}) copy-start(bf16[768,4096]{1,0:T(8,128)(2,1)} %param.17) | copy-start | bytes 18874372
  6.6 9.9 %copy-start.4 = (bf16[4096,512]{1,0:T(8,128)(2,1)S(1)}, bf16[4096,512]{1,0:T(8,128)(2,1)}, u32[]{:S(2)}) copy-start(bf16[4096,512]{1,0:T(8,128)(2,1)} %param.23) | copy-start | bytes 12582916
  20.7 3.4 slice-start
  22.2 2.1 slice-start.1
  22.2 3.2 copy-start.5
  30.5 543.9 %reduce-scatter.2.cloned.1.call-start = ((), (), s32[]{:S(2)}) async-start(), calls=%async_computation.2 | async-start | bytes 7864320 | tf_op jit(solution)/shard_map/reduce_scatter | solution.py:141
  30.8 7.6 %copy-start.6 = (bf16[4096,512]{1,0:T(8,128)(2,1)S(1)}, bf16[4096,512]{1,0:T(8,128)(2,1)}, u32[]{:S(2)}) copy-start(bf16[4096,512]{1,0:T(8,128)(2,1)} %param.19) | copy-start | bytes 12582916
  38.3 10.9 %copy-start.1 = (bf16[3,512]{1,0:T(4,128)(2,1)S(1)}, bf16[3,512]{1,0:T(4,128)(2,1)}, u32[]{:S(2)}) copy-start(bf16[3,512]{1,0:T(4,128)(2,1)} %param.21) | copy-start | bytes 9220
  38.3 10.9 %copy-start.8 = (bf16[128]{0:T(256)(128)(2,1)S(1)}, bf16[128]{0:T(256)(128)(2,1)}, u32[]{:S(2)}) copy-start(bf16[128]{0:T(256)(128)(2,1)} %param.26) | copy-start | bytes 772
  43.9 6.7 %collective-permute-start = (f32[2,512]{1,0:T(2,128)S(1)}, f32[2,512]{1,0:T(2,128)S(1)}, u32[]{:S(2)}, u32[]{:S(2)}) collective-permute-start(f32[2,512]{1,0:T(2,128)S(1)} %slice.41), channel_id=1, source_target_pairs={{0,4},{4,8},{8,12},{12,16},{16,20},{20,24},{24,28},{1,5},{5,9},{9,... | collective-permute-start | bytes 12296 | tf_op jit(solution)/shard_map/ppermute | solution.py:16
  228.2 8.3 %copy-start = (f32[4,2,512,768]{3,2,1,0:T(8,128)S(1)}, f32[4,2,512,768]{3,2,1,0:T(8,128)}, u32[]{:S(2)}) copy-start(f32[4,2,512,768]{3,2,1,0:T(8,128)} %get-tuple-element.298) | copy-start | bytes 37748740 | tf_op jit(solution)/shard_map/cond/branch_1_fun/while
  250.5 8.7 %copy-start = (f32[4,2,512,768]{3,2,1,0:T(8,128)S(1)}, f32[4,2,512,768]{3,2,1,0:T(8,128)}, u32[]{:S(2)}) copy-start(f32[4,2,512,768]{3,2,1,0:T(8,128)} %get-tuple-element.298) | copy-start | bytes 37748740 | tf_op jit(solution)/shard_map/cond/branch_1_fun/while
  274.3 8.7 %copy-start = (f32[4,2,512,768]{3,2,1,0:T(8,128)S(1)}, f32[4,2,512,768]{3,2,1,0:T(8,128)}, u32[]{:S(2)}) copy-start(f32[4,2,512,768]{3,2,1,0:T(8,128)} %get-tuple-element.298) | copy-start | bytes 37748740 | tf_op jit(solution)/shard_map/cond/branch_1_fun/while
  298.2 8.7 %copy-start = (f32[4,2,512,768]{3,2,1,0:T(8,128)S(1)}, f32[4,2,512,768]{3,2,1,0:T(8,128)}, u32[]{:S(2)}) copy-start(f32[4,2,512,768]{3,2,1,0:T(8,128)} %get-tuple-element.298) | copy-start | bytes 37748740 | tf_op jit(solution)/shard_map/cond/branch_1_fun/while
  322.0 8.7 %copy-start = (f32[4,2,512,768]{3,2,1,0:T(8,128)S(1)}, f32[4,2,512,768]{3,2,1,0:T(8,128)}, u32[]{:S(2)}) copy-start(f32[4,2,512,768]{3,2,1,0:T(8,128)} %get-tuple-element.298) | copy-start | bytes 37748740 | tf_op jit(solution)/shard_map/cond/branch_1_fun/while
  345.9 8.7 %copy-start = (f32[4,2,512,768]{3,2,1,0:T(8,128)S(1)}, f32[4,2,512,768]{3,2,1,0:T(8,128)}, u32[]{:S(2)}) copy-start(f32[4,2,512,768]{3,2,1,0:T(8,128)} %get-tuple-element.298) | copy-start | bytes 37748740 | tf_op jit(solution)/shard_map/cond/branch_1_fun/while
  369.7 8.7 %copy-start = (f32[4,2,512,768]{3,2,1,0:T(8,128)S(1)}, f32[4,2,512,768]{3,2,1,0:T(8,128)}, u32[]{:S(2)}) copy-start(f32[4,2,512,768]{3,2,1,0:T(8,128)} %get-tuple-element.298) | copy-start | bytes 37748740 | tf_op jit(solution)/shard_map/cond/branch_1_fun/while
  393.6 8.7 %copy-start = (f32[4,2,512,768]{3,2,1,0:T(8,128)S(1)}, f32[4,2,512,768]{3,2,1,0:T(8,128)}, u32[]{:S(2)}) copy-start(f32[4,2,512,768]{3,2,1,0:T(8,128)} %get-tuple-element.298) | copy-start | bytes 37748740 | tf_op jit(solution)/shard_map/cond/branch_1_fun/while
  417.4 8.7 %copy-start = (f32[4,2,512,768]{3,2,1,0:T(8,128)S(1)}, f32[4,2,512,768]{3,2,1,0:T(8,128)}, u32[]{:S(2)}) copy-start(f32[4,2,512,768]{3,2,1,0:T(8,128)} %get-tuple-element.298) | copy-start | bytes 37748740 | tf_op jit(solution)/shard_map/cond/branch_1_fun/while
  441.2 8.7 %copy-start = (f32[4,2,512,768]{3,2,1,0:T(8,128)S(1)}, f32[4,2,512,768]{3,2,1,0:T(8,128)}, u32[]{:S(2)}) copy-start(f32[4,2,512,768]{3,2,1,0:T(8,128)} %get-tuple-element.298) | copy-start | bytes 37748740 | tf_op jit(solution)/shard_map/cond/branch_1_fun/while
  465.1 8.7 %copy-start = (f32[4,2,512,768]{3,2,1,0:T(8,128)S(1)}, f32[4,2,512,768]{3,2,1,0:T(8,128)}, u32[]{:S(2)}) copy-start(f32[4,2,512,768]{3,2,1,0:T(8,128)} %get-tuple-element.298) | copy-start | bytes 37748740 | tf_op jit(solution)/shard_map/cond/branch_1_fun/while
  488.9 8.7 %copy-start = (f32[4,2,512,768]{3,2,1,0:T(8,128)S(1)}, f32[4,2,512,768]{3,2,1,0:T(8,128)}, u32[]{:S(2)}) copy-start(f32[4,2,512,768]{3,2,1,0:T(8,128)} %get-tuple-element.298) | copy-start | bytes 37748740 | tf_op jit(solution)/shard_map/cond/branch_1_fun/while
  505.3 2.4 copy-start.2
  507.7 2.2 copy-start.7
Sparse Core Ops, SparseCore 0:
  30.6 178.5 all-gather.1
  518.3 56.0 reduce-scatter.1
